TPU v7x, 32 devices: a whole 2x2x4 slice. The times are simulated.
32 devices in a mesh: sp: 8 (over z, y), tp: 4 (over x, core).
Axes of the slice: x: 2, y: 2, z: 4, core: 2. Of those that a mesh axis runs over, the one named last changes fastest.
Arguments:
- resid: bfloat16 [4096, 2048], P(('sp', 'tp')), may hold values from -6 to 6
- query: bfloat16 [4096, 2048], P('sp', 'tp'), may hold values from -6 to 6
- forget_logits: bfloat16 [4096, 2048], P('sp', 'tp'), may hold values from -5 to 5
- forget_margin: float32 [2048], P('tp'), may hold values from 0 to 0.07, as said below
- decay_spike: float32 [4096, 16], P('sp', 'tp'), may hold values from -0.75 to 0
- value_logits: bfloat16 [4096, 2048], P('sp', 'tp'), may hold values from -6 to 6
- output_gate_logits: bfloat16 [4096, 2048], P('sp', 'tp'), may hold values from -6 to 6
- head_norm_scale: float32 [2048], P('tp'), may hold values from 0.1 to 1.9
- output_matrix: bfloat16 [2048, 2048], replicated, may hold values from -0.125 to 0.125
- norm_scale_vector: float32 [2048], replicated, may hold values from 0.1 to 1.9
- routes: int32 [4096, 2], P(('sp', 'tp')), may hold values from 0 to 31, all different within a row; in each aligned block of 128 rows (0 to 127, 128 to 255, ...) at most 16 rows name the same one
- routing_weight: float32 [4096, 2], P(('sp', 'tp')), may hold values from 0.2 to 1
- gate_matrix: bfloat16 [32, 2048, 1024], P(('sp', 'tp')), may hold values from -0.125 to 0.125
- up_matrix: bfloat16 [32, 2048, 1024], P(('sp', 'tp')), may hold values from -0.125 to 0.125
- down_matrix: bfloat16 [32, 1024, 2048], P(('sp', 'tp')), may hold values from -0.1875 to 0.1875
Outputs:
- result: bfloat16 [4096, 2048], P(('sp', 'tp'))
Inputs may be any that keep to these rules, and one draw needn't show every extreme that they name: `routes`: within the rows of one device no expert is named by more than 16 rows; some device names some expert exactly 16 times in every draw. `forget_margin`: Positive.
All inputs are finite; a program needn't handle non-finite values.
Results may differ from a plain program's by a relative error of at most 0.012.
Values may be sent and summed in bfloat16 or wider, within the bound.
A program may use at most 128 MiB of HBM per device.

v0:
```python
import jax
import jax.numpy as jnp
from jax import lax
from jax.experimental import pallas as pl
from jax.experimental.pallas import tpu as pltpu
from jax.sharding import PartitionSpec as P

DK = 128
BLOCK = 64


SPAN = 2 * BLOCK


def spread_dot(left, right, dims):
    return lax.dot_general(left, right, (dims, ((), ())), preferred_element_type=jnp.float32)


def mixing_kernel(
    q_ref, f_ref, m_ref, s_ref, v_ref, g_ref, n_ref, w_ref, r_ref, stream_ref,
    loc_ref, qt_ref, tot_ref, parts_ref, came_ref, answer_ref, back_ref, prior_ref, rows_ref,
    out_ref, matrix_ref,
    ready_sem, came_sem, answer_sem, back_sem, rows_sem, out_sem, matrix_sem,
):
    length, columns = q_ref.shape
    heads = s_ref.shape[0]
    width = columns // heads
    vwidth = v_ref.shape[1] // heads
    count, mates = lax.axis_size("sp"), lax.axis_size("tp")
    me, lane = lax.axis_index("sp"), lax.axis_index("tp")
    part = vwidth // count
    barrier = pltpu.get_barrier_semaphore()
    fetch = pltpu.make_async_copy(w_ref, matrix_ref, matrix_sem)
    fetch.start()
    for d in range(1, count):
        pl.semaphore_signal(
            barrier, inc=1, device_id={"sp": lax.rem(me + d, count)},
            device_id_type=pl.DeviceIdType.MESH,
        )
    for d in range(1, mates):
        pl.semaphore_signal(
            barrier, inc=1, device_id={"tp": lax.rem(lane + d, mates)},
            device_id_type=pl.DeviceIdType.MESH,
        )

    span = min(SPAN, length)
    lower = lax.broadcasted_iota(jnp.int32, (span, span), 0) >= lax.broadcasted_iota(
        jnp.int32, (span, span), 1
    )
    ones = lower.astype(jnp.float32).astype(jnp.bfloat16)
    spot = lax.broadcasted_iota(jnp.int32, (2 * heads, width), 0)

    def one_head(head, carry):
        here = pl.ds(pl.multiple_of(head * width, width), width)
        there = pl.ds(pl.multiple_of(head * vwidth, vwidth), vwidth)
        mine = ((spot == head) | (spot == head + heads)).astype(jnp.float32).astype(jnp.bfloat16)
        margin = m_ref[:, here]
        state = jnp.zeros((vwidth, width), jnp.float32)
        before = jnp.zeros((1, width), jnp.float32)
        for at in range(length // span):
            rows = pl.ds(at * span, span)
            keys = margin * jax.nn.sigmoid(-f_ref[rows, here].astype(jnp.float32))
            spikes = s_ref[:, rows]
            top = spikes.astype(jnp.bfloat16).astype(jnp.float32)
            halves = jnp.concatenate([top, spikes - top], axis=0).astype(jnp.bfloat16)
            decay = jnp.log1p(-keys) + spread_dot(halves, mine, ((0,), (0,)))
            high = decay.astype(jnp.bfloat16)
            low = (decay - high.astype(jnp.float32)).astype(jnp.bfloat16)
            both = spread_dot(ones, jnp.concatenate([high, low], axis=1), ((1,), (0,)))
            cum = both[:, :width] + both[:, width:]
            middle = cum[span // 2 - 1 : span // 2, :]
            last = cum[span - 1 : span, :]
            down = jnp.exp(cum - middle)
            up = jnp.exp(middle - cum)
            query = q_ref[rows, here].astype(jnp.float32) * DK ** (-0.5)
            logits = v_ref[rows, there].astype(jnp.float32)
            value = (logits * jax.nn.sigmoid(logits)).astype(jnp.bfloat16)
            near = query * down
            rise = keys * up
            score = spread_dot(
                near.astype(jnp.bfloat16), rise.astype(jnp.bfloat16), ((1,), (1,))
            )
            score = jnp.where(lower, score, 0.0).astype(jnp.bfloat16)
            result = spread_dot(score, value, ((1,), (0,)))
            reach = near * jnp.exp(middle)
            if at > 0:
                result = result + spread_dot(
                    reach.astype(jnp.bfloat16), state.astype(jnp.bfloat16), ((1,), (1,))
                )
            loc_ref[rows, there] = result
            qt_ref[rows, here] = (reach * jnp.exp(before)).astype(jnp.bfloat16)
            kept = (rise * jnp.exp(last - middle)).astype(jnp.bfloat16)
            state = jnp.exp(last) * state + spread_dot(value, kept, ((0,), (0,)))
            before = before + last
        for j in range(count):
            parts_ref[j, head, 0:part, :] = state[j * part : (j + 1) * part, :].astype(
                jnp.bfloat16
            )
        tot_ref[pl.ds(head, 1), :] = before
        return carry

    lax.fori_loop(0, heads, one_head, 0)
    total = tot_ref[...]
    top = total.astype(jnp.bfloat16).astype(jnp.float32)
    deep = parts_ref.shape[2]
    filler = [jnp.zeros((deep - 2 * heads, width), jnp.float32)] if deep > 2 * heads else []
    logs = jnp.concatenate([top, total - top] + filler, axis=0).astype(jnp.bfloat16)
    for j in range(count):
        parts_ref[j, heads] = logs

    pl.semaphore_wait(barrier, count + mates - 2)

    def exchange(source, target, send_sem, recv_sem):
        copies = []
        for d in range(1, count):
            peer = lax.rem(me + d, count)
            copy = pltpu.make_async_remote_copy(
                src_ref=source.at[peer], dst_ref=target.at[me],
                send_sem=send_sem.at[d], recv_sem=recv_sem.at[d],
                device_id={"sp": peer}, device_id_type=pl.DeviceIdType.MESH,
            )
            copy.start()
            copies.append(copy)
        target[me] = source[me]
        for copy in copies:
            copy.wait_recv()
        return copies

    first = exchange(parts_ref, came_ref, ready_sem, came_sem)
    so_far = [jnp.zeros((part, width), jnp.float32) for _ in range(heads)]
    for i in range(count):
        marks = came_ref[i, heads].astype(jnp.float32)
        fade = jnp.exp(marks[0:heads, :] + marks[heads : 2 * heads, :])
        for h in range(heads):
            answer_ref[i, h] = so_far[h].astype(jnp.bfloat16)
            piece = came_ref[i, h].astype(jnp.float32)[0:part, :]
            so_far[h] = fade[h : h + 1, :] * so_far[h] + piece
    second = exchange(answer_ref, back_ref, answer_sem, back_sem)
    for i in range(count):
        for h in range(heads):
            prior_ref[h, i * part : (i + 1) * part, :] = back_ref[i, h].astype(jnp.float32)

    own_rows = length // mates
    wide = heads * vwidth
    third = []
    mine_at = pl.ds(pl.multiple_of(lane * wide, wide), wide)
    for d in range(1, mates + 1):
        peer = lax.rem(lane + d, mates)
        rows = pl.ds(pl.multiple_of(peer * own_rows, own_rows), own_rows)
        pieces = []
        for h in range(heads):
            there = slice(h * vwidth, (h + 1) * vwidth)
            full = loc_ref[rows, there] + spread_dot(
                qt_ref[rows, h * width : (h + 1) * width],
                prior_ref[h].astype(jnp.bfloat16), ((1,), (1,)),
            )
            square = jnp.mean(full * full, axis=1, keepdims=True)
            gate = g_ref[rows, there].astype(jnp.float32)
            scaled = full * lax.rsqrt(square + 1e-06) * n_ref[:, there]
            pieces.append((scaled * (gate * jax.nn.sigmoid(gate))).astype(jnp.bfloat16))
        gated = jnp.concatenate(pieces, axis=1)
        if d == mates:
            out_ref[:, mine_at] = gated
        else:
            rows_ref[d - 1] = gated
            copy = pltpu.make_async_remote_copy(
                src_ref=rows_ref.at[d - 1], dst_ref=out_ref.at[:, mine_at],
                send_sem=rows_sem.at[d], recv_sem=out_sem.at[d],
                device_id={"tp": peer}, device_id_type=pl.DeviceIdType.MESH,
            )
            copy.start()
            third.append(copy)
    for copy in third:
        copy.wait_recv()
    fetch.wait()
    model = matrix_ref.shape[1]
    tile = model // 4
    for at in range(4):
        cols = slice(at * tile, (at + 1) * tile)
        mixed = jnp.dot(
            out_ref[...], matrix_ref[:, cols], preferred_element_type=jnp.float32
        )
        stream_ref[:, cols] = (r_ref[:, cols].astype(jnp.float32) + mixed).astype(jnp.bfloat16)
    for copy in first + second + third:
        copy.wait_send()


def gated_arrivals(query, forget_logits, margin, spike, value_logits, gate_logits, head_scale, matrix, resid):
    length, columns = query.shape
    heads = spike.shape[1]
    width = columns // heads
    wide = value_logits.shape[1]
    vwidth = wide // heads
    count, mates = lax.axis_size("sp"), lax.axis_size("tp")
    part = vwidth // count
    deep = max(part, 2 * heads)
    rows = length // mates
    vmem = pl.BlockSpec(memory_space=pltpu.VMEM)
    return pl.pallas_call(
        mixing_kernel,
        in_specs=[vmem] * 7 + [pl.BlockSpec(memory_space=pl.ANY), vmem],
        out_specs=vmem,
        out_shape=jax.ShapeDtypeStruct(resid.shape, jnp.bfloat16),
        scratch_shapes=[
            pltpu.VMEM((length, wide), jnp.float32),
            pltpu.VMEM((length, columns), jnp.bfloat16),
            pltpu.VMEM((heads, width), jnp.float32),
            pltpu.VMEM((count, heads + 1, deep, width), jnp.bfloat16),
            pltpu.VMEM((count, heads + 1, deep, width), jnp.bfloat16),
            pltpu.VMEM((count, heads, part, width), jnp.bfloat16),
            pltpu.VMEM((count, heads, part, width), jnp.bfloat16),
            pltpu.VMEM((heads, vwidth, width), jnp.float32),
            pltpu.VMEM((mates - 1, rows, wide), jnp.bfloat16),
            pltpu.VMEM((rows, mates * wide), jnp.bfloat16),
            pltpu.VMEM(matrix.shape, matrix.dtype),
            pltpu.SemaphoreType.DMA((count,)),
            pltpu.SemaphoreType.DMA((count,)),
            pltpu.SemaphoreType.DMA((count,)),
            pltpu.SemaphoreType.DMA((count,)),
            pltpu.SemaphoreType.DMA((mates,)),
            pltpu.SemaphoreType.DMA((mates,)),
            pltpu.SemaphoreType.DMA,
        ],
        compiler_params=pltpu.CompilerParams(collective_id=0, has_side_effects=True),
    )(
        query, forget_logits, margin[None, :], spike.T, value_logits, gate_logits,
        head_scale[None, :], matrix, resid,
    )


def row_norm(stream, norm_scale_vector):
    values = stream.astype(jnp.float32)
    square = jnp.mean(values * values, axis=1, keepdims=True)
    return (values * lax.rsqrt(square + 1e-06) * norm_scale_vector[None, :]).astype(jnp.bfloat16)


def expert_block(slot_rows, gate_matrix, up_matrix, down_matrix):
    gate_part = jnp.einsum(
        "...ecd,edf->...ecf", slot_rows, gate_matrix, preferred_element_type=jnp.float32
    )
    up_part = jnp.einsum(
        "...ecd,edf->...ecf", slot_rows, up_matrix, preferred_element_type=jnp.float32
    )
    hidden = (jax.nn.silu(gate_part) * up_part).astype(jnp.bfloat16)
    return jnp.einsum(
        "...ecf,efd->...ecd", hidden, down_matrix, preferred_element_type=jnp.float32
    ).astype(jnp.bfloat16)


def body(
    resid,
    query,
    forget_logits,
    forget_margin,
    decay_spike,
    value_logits,
    output_gate_logits,
    head_norm_scale,
    output_matrix,
    norm_scale_vector,
    routes,
    routing_weight,
    gate_matrix,
    up_matrix,
    down_matrix,
):
    stream = gated_arrivals(
        query, forget_logits, forget_margin, decay_spike, value_logits,
        output_gate_logits, head_norm_scale, output_matrix, resid,
    )
    normed = row_norm(stream, norm_scale_vector)
    row_count = routes.shape[0]
    top_count = routes.shape[1]
    model_width = normed.shape[1]
    per_device = gate_matrix.shape[0]
    devices = lax.axis_size("sp") * lax.axis_size("tp")
    experts = per_device * devices
    capacity = 2 * row_count * top_count // experts
    flat_routes = routes.reshape(-1)
    member = (flat_routes[:, None] == jnp.arange(experts, dtype=jnp.int32)[None, :]).astype(
        jnp.int32
    )
    slot_rank = jnp.sum(jnp.cumsum(member, axis=0) * member, axis=1) - 1
    position_entries = flat_routes * capacity + slot_rank
    select = (
        position_entries[:, None] == jnp.arange(experts * capacity, dtype=jnp.int32)[None, :]
    ).astype(jnp.bfloat16)
    select = select.reshape(row_count, top_count, experts * capacity)
    dispatch = jnp.sum(select, axis=1)
    packed = lax.dot_general(
        dispatch, normed, (((0,), (0,)), ((), ())), preferred_element_type=jnp.float32
    ).astype(jnp.bfloat16)
    direct = packed.reshape(devices, per_device, capacity, model_width)
    answers = expert_block(
        lax.all_to_all(direct, ("sp", "tp"), split_axis=0, concat_axis=0, tiled=True),
        gate_matrix,
        up_matrix,
        down_matrix,
    )
    returned = lax.all_to_all(answers, ("sp", "tp"), split_axis=0, concat_axis=0, tiled=True)
    returned_rows = returned.reshape(experts * capacity, model_width)
    combined = stream.astype(jnp.float32)
    for pick_index in range(top_count):
        picked = jnp.dot(
            select[:, pick_index, :], returned_rows, preferred_element_type=jnp.float32
        )
        combined = combined + routing_weight[:, pick_index : pick_index + 1] * picked
    return combined.astype(jnp.bfloat16)


def solution(mesh):
    return jax.shard_map(
        body,
        mesh=mesh,
        in_specs=(
            P(("sp", "tp"), None),
            P("sp", "tp"),
            P("sp", "tp"),
            P("tp"),
            P("sp", "tp"),
            P("sp", "tp"),
            P("sp", "tp"),
            P("tp"),
            P(),
            P(),
            P(("sp", "tp"), None),
            P(("sp", "tp"), None),
            P(("sp", "tp"), None, None),
            P(("sp", "tp"), None, None),
            P(("sp", "tp"), None, None),
        ),
        out_specs=P(("sp", "tp"), None),
        check_vma=False,
    )
```

profile of v0, /device:TPU:7, one launch (start us, length us, event | category | flops | bytes accessed | tf_op | source)
XLA Modules:
  0.0 154.4 jit_solution(3101675278983470932)
XLA Ops:
  0.0 0.8 copy.31
  0.8 0.1 eq.44
  0.9 0.1 eq.40
  1.1 0.6 reduce-window.6
  1.7 0.2 slice_reduce_fusion
  1.9 0.1 fusion.41
  2.0 0.1 sub.7
  2.2 0.1 copy.34
  2.2 0.7 multiply_add_fusion
  2.9 0.1 convert_reduce_fusion
  3.1 0.0 copy-start.1
  3.1 27.8 %shard_map.145 = bf16[128,2048]{1,0:T(8,128)(2,1)} custom-call(bf16[512,512]{1,0:T(8,128)(2,1)} %q_ref.1, bf16[512,512]{1,0:T(8,128)(2,1)} %f_ref.1, f32[1,512]{1,0:T(1,128)} %bitcast.117, f32[4,512]{1,0:T(4,128)} %bitcast.116, bf16[512,512]{1,0:T(8,128)(2,1)} %v_ref.1, bf16[512,512]{1,0:T(8,128)(2,1)} %g_ref.1, f32[1,512]{1,0:T(1,128)} %bitcast.118, ...), custom_call_target="tpu_custom_call" | custom-call | tf_op jit(solution)/shard_map/pallas_call | solution.py:199
  30.9 1.2 fusion.30
  32.1 0.0 copy-done.1
  32.1 1.8 %convolution_convert_fusion = bf16[512,2048]{1,0:T(8,128)(2,1)S(1)} fusion(bf16[128,512]{1,0:T(8,128)(2,1)S(1)} %convert_reduce_fusion, bf16[128,2048]{1,0:T(8,128)(2,1)} %shard_map.145, f32[2048]{0:T(1024)S(1)} %copy-done.1, f32[128]{0:T(128)S(1)} %add_rsqrt_fusion), kind=kOutput, calls=%fused_computation.7 | convolution fusion | flops 270532608 | bytes 2761216 | tf_op jit(solution)/shard_map/dot_general | solution.py:290
  34.0 0.0 copy-start.3
  34.0 52.2 %all_to_all.10 = bf16[32,1,16,2048]{3,2,1,0:T(8,128)(2,1)S(1)} all-to-all(bf16[32,1,16,2048]{3,2,1,0:T(8,128)(2,1)S(1)} %bitcast.115), channel_id=1, replica_groups=mesh['sp'=8,'tp'=4] {'sp','tp'}, dimensions={0} | all-to-all | bytes 4194304 | tf_op jit(solution)/shard_map/all_to_all | solution.py:295
  86.2 0.0 copy-done.3
  86.2 3.7 %fusion.2 = f32[32,16,1024]{2,1,0:T(8,128)} fusion(bf16[1,2048,1024]{2,1,0:T(8,128)(2,1)S(1)} %copy-done.3, bf16[32,1,16,2048]{3,2,1,0:T(8,128)(2,1)S(1)} %all_to_all.10), kind=kOutput, calls=%fused_computation.2 | convolution fusion | flops 2147483648 | bytes 8388608 | tf_op jit(solution)/shard_map/...ecd,edf->...ecf/dot_general | solution.py:241
  90.0 10.1 %fusion.9 = bf16[32,1,16,2048]{3,2,1,0:T(8,128)(2,1)} fusion(bf16[1,1024,2048]{2,1,0:T(8,128)(2,1)} %param.29, f32[32,16,1024]{2,1,0:T(8,128)} %fusion.2, bf16[1,2048,1024]{2,1,0:T(8,128)(2,1)} %param.27, bf16[32,1,16,2048]{3,2,1,0:T(8,128)(2,1)S(1)} %all_to_all.10), kind=kOutput, calls=%fused_computation.8 | convolution fusion | flops 4299161600 | bytes 14680064 | tf_op jit(solution)/shard_map/...ecf,efd->...ecd/dot_general | solution.py:245
  100.0 0.0 copy-start.2
  100.0 0.0 copy-start
  100.0 4.6 %all-to-all-start.1 = ((bf16[32,1,16,2048]{3,2,1,0:T(8,128)(2,1)}), bf16[32,1,16,2048]{3,2,1,0:T(8,128)(2,1)S(1)}, u32[]{:S(2)}, u32[]{:S(2)}) async-start(bf16[32,1,16,2048]{3,2,1,0:T(8,128)(2,1)} %fusion.9), calls=%async_computation.1 | async-start | bytes 4194304 | tf_op jit(solution)/shard_map/all_to_all | solution.py:300
  104.6 0.0 copy-done.2
  104.7 0.1 iota_compare_fusion
  104.8 47.8 %all-to-all-done.1 = bf16[32,1,16,2048]{3,2,1,0:T(8,128)(2,1)S(1)} async-done(((bf16[32,1,16,2048]{3,2,1,0:T(8,128)(2,1)}), bf16[32,1,16,2048]{3,2,1,0:T(8,128)(2,1)S(1)}, u32[]{:S(2)}, u32[]{:S(2)}) %all-to-all-start.1) | async-done | bytes 2097184 | tf_op jit(solution)/shard_map/all_to_all | solution.py:300
  152.6 0.0 copy-done
  152.6 0.5 fusion.13
  153.1 1.3 fusion.14
  (6 shorter events, 0.1 us)
Async XLA Ops:
  3.1 29.1 %copy-start.1 = (f32[2048]{0:T(1024)S(1)}, f32[2048]{0:T(1024)}, u32[]{:S(2)}) copy-start(f32[2048]{0:T(1024)} %param.24) | copy-start | bytes 24580
  34.0 52.3 %copy-start.3 = (bf16[1,2048,1024]{2,1,0:T(8,128)(2,1)S(1)}, bf16[1,2048,1024]{2,1,0:T(8,128)(2,1)}, u32[]{:S(2)}) copy-start(bf16[1,2048,1024]{2,1,0:T(8,128)(2,1)} %param.28) | copy-start | bytes 12582916
  100.0 4.6 %copy-start.2 = (f32[128,2]{0,1:T(2,128)S(1)}, f32[128,2]{0,1:T(2,128)}, u32[]{:S(2)}) copy-start(f32[128,2]{0,1:T(2,128)} %param.26) | copy-start | bytes 3076
  100.0 52.5 %copy-start = (bf16[128,2048]{1,0:T(8,128)(2,1)S(1)}, bf16[128,2048]{1,0:T(8,128)(2,1)}, u32[]{:S(2)}) copy-start(bf16[128,2048]{1,0:T(8,128)(2,1)} %shard_map.145) | copy-start | bytes 1572868
  100.0 52.5 %all-to-all-start.1 = ((bf16[32,1,16,2048]{3,2,1,0:T(8,128)(2,1)}), bf16[32,1,16,2048]{3,2,1,0:T(8,128)(2,1)S(1)}, u32[]{:S(2)}, u32[]{:S(2)}) async-start(bf16[32,1,16,2048]{3,2,1,0:T(8,128)(2,1)} %fusion.9), calls=%async_computation.1 | async-start | bytes 4194304 | tf_op jit(solution)/shard_map/all_to_all | solution.py:300
where the time goes:
time: 156 us; the launch traced here: 154 us
  blocking collectives  52.2 us (33%)
  waiting for transfers between devices  47.8 us (31%)
  Pallas kernels  27.8 us (18%)
  matrix products  17.4 us (11%)
  starting transfers between devices  4.61 us (3%)
  other arithmetic  2.93 us (2%)
    all_to_all x1, blocking collectives, body(): lax.all_to_all(direct, ('sp', 'tp'), split_axis=0, concat_axis=0, tiled=T...  52.2 us
    all_to_all x1, waiting for transfers between devices, body(): lax.all_to_all(answers, ('sp', 'tp'), split_axis=0, concat_axis=0, tiled=...  47.8 us
    pallas_call x1, Pallas kernels, gated_arrivals(): pl.pallas_call(mixing_kernel, in_specs=[vmem] * 7 + [pl.BlockSpec(memory_...  27.8 us
    dot_general x1, matrix products, expert_block(): jnp.einsum('...ecf,efd->...ecd', hidden, down_matrix, preferred_element_t...  10.1 us
    all_to_all x1, starting transfers between devices, body(): lax.all_to_all(answers, ('sp', 'tp'), split_axis=0, concat_axis=0, tiled=...  4.61 us
    dot_general x1, matrix products, expert_block(): jnp.einsum('...ecd,edf->...ecf', slot_rows, up_matrix, preferred_element_...  3.73 us
  transfers between devices with their start and end apart: 1, of which 1 were waited for; matrix products, arithmetic and copies ran while one was open for 0% of the time, Pallas kernels for 0%

commit v1 on v0

--- a/solution.py
+++ b/solution.py
@@ -228,23 +228,279 @@
     )
 
 
-def row_norm(stream, norm_scale_vector):
-    values = stream.astype(jnp.float32)
+CHUNKS = 2
+TILE = 256
+SLOTS = 16
+
+
+def tile_of(extent):
+    return min(TILE, extent)
+
+
+def expert_kernel(
+    stream_ref, scale_ref, routes_ref, weight_ref, gate_ref, up_ref, down_ref, out_ref,
+    normed_ref, meta_ref, pack_ref, came_ref, hidden_ref, answer_ref, back_ref, part_ref, far_ref, total_ref,
+    gate_vmem, up_vmem, down_vmem,
+    load_sem, meta_send, meta_recv, over_send, over_recv, out_send, out_recv,
+    ret_send, ret_recv, home_send, home_recv,
+):
+    rows, model = stream_ref.shape
+    hidden = gate_vmem.shape[1]
+    count, mates = lax.axis_size("sp"), lax.axis_size("tp")
+    me, lane = lax.axis_index("sp"), lax.axis_index("tp")
+    near = count // 2
+    side = me // near
+    peers = near * mates
+    spot = (me - side * near) * mates + lane
+    mirror = lax.rem(me + near, count)
+    slots = came_ref.shape[1] // peers
+    experts = peers * 2
+    wide = model // CHUNKS
+
+    loads = []
+    for at, (source, target) in enumerate(
+        ((gate_ref, gate_vmem), (up_ref, up_vmem), (down_ref, down_vmem))
+    ):
+        copy = pltpu.make_async_copy(source.at[0], target, load_sem.at[at])
+        copy.start()
+        loads.append(copy)
+
+    def place(d):
+        other = lax.rem(spot + d, peers)
+        return other, {"sp": side * near + other // mates, "tp": lax.rem(other, mates)}
+
+    barrier = pltpu.get_barrier_semaphore()
+    pl.semaphore_signal(
+        barrier, inc=1, device_id={"sp": mirror}, device_id_type=pl.DeviceIdType.MESH
+    )
+
+    def greet(d, carry):
+        pl.semaphore_signal(
+            barrier, inc=1, device_id=place(d)[1], device_id_type=pl.DeviceIdType.MESH
+        )
+        return carry
+
+    lax.fori_loop(1, peers, greet, 0)
+
+    values = stream_ref[...].astype(jnp.float32)
     square = jnp.mean(values * values, axis=1, keepdims=True)
-    return (values * lax.rsqrt(square + 1e-06) * norm_scale_vector[None, :]).astype(jnp.bfloat16)
-
-
-def expert_block(slot_rows, gate_matrix, up_matrix, down_matrix):
-    gate_part = jnp.einsum(
-        "...ecd,edf->...ecf", slot_rows, gate_matrix, preferred_element_type=jnp.float32
-    )
-    up_part = jnp.einsum(
-        "...ecd,edf->...ecf", slot_rows, up_matrix, preferred_element_type=jnp.float32
-    )
-    hidden = (jax.nn.silu(gate_part) * up_part).astype(jnp.bfloat16)
-    return jnp.einsum(
-        "...ecf,efd->...ecd", hidden, down_matrix, preferred_element_type=jnp.float32
-    ).astype(jnp.bfloat16)
+    normed_ref[0] = (values * lax.rsqrt(square + 1e-06) * scale_ref[...]).astype(jnp.bfloat16)
+
+    routes = routes_ref[...]
+    named = lax.broadcasted_iota(jnp.int32, (experts, rows), 0)
+    hits = [named == routes[k : k + 1, :] for k in range(2)]
+    member = (hits[0] | hits[1]).astype(jnp.float32).astype(jnp.bfloat16)
+    earlier = (
+        lax.broadcasted_iota(jnp.int32, (rows, rows), 0)
+        < lax.broadcasted_iota(jnp.int32, (rows, rows), 1)
+    ).astype(jnp.float32).astype(jnp.bfloat16)
+    ranks = spread_dot(member, earlier, ((1,), (0,)))
+    for k in range(2):
+        rank = jnp.sum(jnp.where(hits[k], ranks, 0.0), axis=0, keepdims=True)
+        meta_ref[0, k : k + 1, :] = routes[k : k + 1, :].astype(jnp.float32) * slots + rank
+        meta_ref[0, 2 + k : 3 + k, :] = weight_ref[k : k + 1, :]
+    meta_ref[0, 4:8, :] = jnp.zeros((4, rows), jnp.float32)
+
+    pl.semaphore_wait(barrier, peers)
+
+    def across(source, target, send_sem, recv_sem):
+        return pltpu.make_async_remote_copy(
+            src_ref=source, dst_ref=target, send_sem=send_sem, recv_sem=recv_sem,
+            device_id={"sp": mirror}, device_id_type=pl.DeviceIdType.MESH,
+        )
+
+    note = across(meta_ref.at[0], meta_ref.at[1], meta_send, meta_recv)
+    note.start()
+    over = []
+    for c in range(CHUNKS):
+        cols = pl.ds(c * wide, wide)
+        copy = across(
+            normed_ref.at[0, :, cols], normed_ref.at[1, :, cols], over_send.at[c], over_recv.at[c]
+        )
+        copy.start()
+        over.append(copy)
+
+    def mine_at():
+        return pl.ds(pl.multiple_of(spot * slots, slots), slots)
+
+    def parcel(source, target, block, cols, turn, d, send_sem, recv_sem):
+        other, device = place(d)
+        there = pl.ds(pl.multiple_of(other * slots, slots), slots)
+        return pltpu.make_async_remote_copy(
+            src_ref=source.at[block, there, cols], dst_ref=target.at[block, mine_at(), cols],
+            send_sem=send_sem.at[turn, d], recv_sem=recv_sem.at[turn, d],
+            device_id=device, device_id_type=pl.DeviceIdType.MESH,
+        )
+
+    def spread(source, target, block, cols, turn, send_sem, recv_sem):
+        def step(d, carry):
+            parcel(source, target, block, cols, turn, d, send_sem, recv_sem).start()
+            return carry
+
+        lax.fori_loop(1, peers, step, 0)
+        target[block, mine_at(), cols] = source[block, mine_at(), cols]
+
+    def arrive(source, target, block, cols, turn, send_sem, recv_sem):
+        def step(d, carry):
+            parcel(source, target, block, cols, turn, d, send_sem, recv_sem).wait_recv()
+            return carry
+
+        lax.fori_loop(1, peers, step, 0)
+
+    def depart(source, target, block, cols, turn, send_sem, recv_sem):
+        def step(d, carry):
+            parcel(source, target, block, cols, turn, d, send_sem, recv_sem).wait_send()
+            return carry
+
+        lax.fori_loop(1, peers, step, 0)
+
+    lot = lax.broadcasted_iota(jnp.int32, (peers * slots, rows), 0).astype(jnp.float32)
+
+    def picks(block):
+        first = (side * peers * slots).astype(jnp.float32)
+        return [lot == meta_ref[block, k : k + 1, :] - first for k in range(2)]
+
+    def pack(block, cols):
+        chosen = picks(block)
+        select = (chosen[0] | chosen[1]).astype(jnp.float32).astype(jnp.bfloat16)
+        extent = cols.size
+        step = tile_of(extent)
+        for at in range(extent // step):
+            here = pl.ds(cols.start + at * step, step)
+            pack_ref[block, :, here] = spread_dot(
+                select, normed_ref[block, :, here], ((1,), (0,))
+            ).astype(jnp.bfloat16)
+
+    def enter(block):
+        def step(at, carry):
+            here = pl.ds(pl.multiple_of(at * tile_of(hidden), tile_of(hidden)), tile_of(hidden))
+            gate = spread_dot(came_ref[block], gate_vmem[:, here], ((1,), (0,)))
+            up = spread_dot(came_ref[block], up_vmem[:, here], ((1,), (0,)))
+            hidden_ref[:, here] = (gate * jax.nn.sigmoid(gate) * up).astype(jnp.bfloat16)
+            return carry
+
+        lax.fori_loop(0, hidden // tile_of(hidden), step, 0)
+
+    def leave(block, cols):
+        size = tile_of(cols.size)
+
+        def step(at, carry):
+            here = pl.ds(pl.multiple_of(cols.start + at * size, size), size)
+            answer_ref[block, :, here] = spread_dot(
+                hidden_ref[...], down_vmem[:, here], ((1,), (0,))
+            ).astype(jnp.bfloat16)
+            return carry
+
+        lax.fori_loop(0, cols.size // size, step, 0)
+
+    def weights(block):
+        chosen = picks(block)
+        load = jnp.where(chosen[0], meta_ref[block, 2:3, :], 0.0) + jnp.where(
+            chosen[1], meta_ref[block, 3:4, :], 0.0
+        )
+        high = load.astype(jnp.bfloat16)
+        return high, (load - high.astype(jnp.float32)).astype(jnp.bfloat16)
+
+    def gather(block, here, high, low):
+        piece = back_ref[block, :, here]
+        return spread_dot(high, piece, ((0,), (0,))) + spread_dot(low, piece, ((0,), (0,)))
+
+    whole = pl.ds(0, model)
+    parts = [pl.ds(c * wide, wide) for c in range(CHUNKS)]
+
+    pack(0, whole)
+    spread(pack_ref, came_ref, 0, whole, 0, out_send, out_recv)
+    for copy in loads:
+        copy.wait()
+    arrive(pack_ref, came_ref, 0, whole, 0, out_send, out_recv)
+    enter(0)
+    leave(0, whole)
+    spread(answer_ref, back_ref, 0, whole, 0, ret_send, ret_recv)
+
+    note.wait_recv()
+    for c in range(CHUNKS):
+        over[c].wait_recv()
+        pack(1, parts[c])
+        spread(pack_ref, came_ref, 1, parts[c], 1 + c, out_send, out_recv)
+    for c in range(CHUNKS):
+        arrive(pack_ref, came_ref, 1, parts[c], 1 + c, out_send, out_recv)
+    enter(1)
+    for c in range(CHUNKS):
+        leave(1, parts[c])
+        spread(answer_ref, back_ref, 1, parts[c], 1 + c, ret_send, ret_recv)
+
+    home = []
+    high, low = weights(1)
+    for c in range(CHUNKS):
+        arrive(answer_ref, back_ref, 1, parts[c], 1 + c, ret_send, ret_recv)
+        size = tile_of(wide)
+        for at in range(wide // size):
+            here = pl.ds(c * wide + at * size, size)
+            part_ref[:, here] = gather(1, here, high, low).astype(jnp.bfloat16)
+        copy = across(
+            part_ref.at[:, parts[c]], far_ref.at[:, parts[c]], home_send.at[c], home_recv.at[c]
+        )
+        copy.start()
+        home.append(copy)
+
+    arrive(answer_ref, back_ref, 0, whole, 0, ret_send, ret_recv)
+    high, low = weights(0)
+    for at in range(model // tile_of(model)):
+        here = pl.ds(at * tile_of(model), tile_of(model))
+        total_ref[:, here] = stream_ref[:, here].astype(jnp.float32) + gather(0, here, high, low)
+    for c in range(CHUNKS):
+        home[c].wait_recv()
+        out_ref[:, parts[c]] = (
+            total_ref[:, parts[c]] + far_ref[:, parts[c]].astype(jnp.float32)
+        ).astype(jnp.bfloat16)
+
+    note.wait_send()
+    for copy in over + home:
+        copy.wait_send()
+    depart(pack_ref, came_ref, 0, whole, 0, out_send, out_recv)
+    depart(answer_ref, back_ref, 0, whole, 0, ret_send, ret_recv)
+    for c in range(CHUNKS):
+        depart(pack_ref, came_ref, 1, parts[c], 1 + c, out_send, out_recv)
+        depart(answer_ref, back_ref, 1, parts[c], 1 + c, ret_send, ret_recv)
+
+
+def routed_experts(stream, scale, routes, weight, gate_matrix, up_matrix, down_matrix):
+    rows, model = stream.shape
+    hidden = gate_matrix.shape[2]
+    peers = lax.axis_size("sp") // 2 * lax.axis_size("tp")
+    capacity = 2 * rows * routes.shape[1] // (2 * peers * gate_matrix.shape[0])
+    slots = -(-capacity // SLOTS) * SLOTS
+    vmem = pl.BlockSpec(memory_space=pltpu.VMEM)
+    anywhere = pl.BlockSpec(memory_space=pl.ANY)
+    blocks = pltpu.VMEM((2, peers * slots, model), jnp.bfloat16)
+    pair = pltpu.SemaphoreType.DMA((CHUNKS,))
+    fan = pltpu.SemaphoreType.DMA((1 + CHUNKS, peers))
+    return pl.pallas_call(
+        expert_kernel,
+        in_specs=[vmem] * 4 + [anywhere] * 3,
+        out_specs=vmem,
+        out_shape=jax.ShapeDtypeStruct((rows, model), jnp.bfloat16),
+        scratch_shapes=[
+            pltpu.VMEM((2, rows, model), jnp.bfloat16),
+            pltpu.VMEM((2, 8, rows), jnp.float32),
+            blocks,
+            blocks,
+            pltpu.VMEM((peers * slots, hidden), jnp.bfloat16),
+            blocks,
+            blocks,
+            pltpu.VMEM((rows, model), jnp.bfloat16),
+            pltpu.VMEM((rows, model), jnp.bfloat16),
+            pltpu.VMEM((rows, model), jnp.float32),
+            pltpu.VMEM((model, hidden), jnp.bfloat16),
+            pltpu.VMEM((model, hidden), jnp.bfloat16),
+            pltpu.VMEM((hidden, model), jnp.bfloat16),
+            pltpu.SemaphoreType.DMA((3,)),
+            pltpu.SemaphoreType.DMA,
+            pltpu.SemaphoreType.DMA,
+            pair, pair, fan, fan, fan, fan, pair, pair,
+        ],
+        compiler_params=pltpu.CompilerParams(collective_id=1, has_side_effects=True),
+    )(stream, scale[None, :], routes.T, weight.T, gate_matrix, up_matrix, down_matrix)
 
 
 def body(
@@ -268,44 +524,9 @@
         query, forget_logits, forget_margin, decay_spike, value_logits,
         output_gate_logits, head_norm_scale, output_matrix, resid,
     )
-    normed = row_norm(stream, norm_scale_vector)
-    row_count = routes.shape[0]
-    top_count = routes.shape[1]
-    model_width = normed.shape[1]
-    per_device = gate_matrix.shape[0]
-    devices = lax.axis_size("sp") * lax.axis_size("tp")
-    experts = per_device * devices
-    capacity = 2 * row_count * top_count // experts
-    flat_routes = routes.reshape(-1)
-    member = (flat_routes[:, None] == jnp.arange(experts, dtype=jnp.int32)[None, :]).astype(
-        jnp.int32
+    return routed_experts(
+        stream, norm_scale_vector, routes, routing_weight, gate_matrix, up_matrix, down_matrix
     )
-    slot_rank = jnp.sum(jnp.cumsum(member, axis=0) * member, axis=1) - 1
-    position_entries = flat_routes * capacity + slot_rank
-    select = (
-        position_entries[:, None] == jnp.arange(experts * capacity, dtype=jnp.int32)[None, :]
-    ).astype(jnp.bfloat16)
-    select = select.reshape(row_count, top_count, experts * capacity)
-    dispatch = jnp.sum(select, axis=1)
-    packed = lax.dot_general(
-        dispatch, normed, (((0,), (0,)), ((), ())), preferred_element_type=jnp.float32
-    ).astype(jnp.bfloat16)
-    direct = packed.reshape(devices, per_device, capacity, model_width)
-    answers = expert_block(
-        lax.all_to_all(direct, ("sp", "tp"), split_axis=0, concat_axis=0, tiled=True),
-        gate_matrix,
-        up_matrix,
-        down_matrix,
-    )
-    returned = lax.all_to_all(answers, ("sp", "tp"), split_axis=0, concat_axis=0, tiled=True)
-    returned_rows = returned.reshape(experts * capacity, model_width)
-    combined = stream.astype(jnp.float32)
-    for pick_index in range(top_count):
-        picked = jnp.dot(
-            select[:, pick_index, :], returned_rows, preferred_element_type=jnp.float32
-        )
-        combined = combined + routing_weight[:, pick_index : pick_index + 1] * picked
-    return combined.astype(jnp.bfloat16)
 
 
 def solution(mesh):

time: 156 us -> 133 us (0.85)
  Pallas kernels: 27.8 us -> 129 us
  blocking collectives: 52.2 us -> 0 us
  waiting for transfers between devices: 47.8 us -> 0 us
  matrix products: 17.4 us -> 0 us
  starting transfers between devices: 4.61 us -> 0 us
  other arithmetic: 2.93 us -> 0 us
    pallas_call x0 -> x1, Pallas kernels: none -> 102 us  [routed_experts(): pl.pallas_call(expert_kernel, in_specs=[vmem] * 4 + [anywhere] * 3, out_s...]
    all_to_all x1 -> x0, blocking collectives: 52.2 us -> none  [body(): lax.all_to_all(direct, ('sp', 'tp'), split_axis=0, concat_axis=0, tiled=T...]
    all_to_all x1 -> x0, waiting for transfers between devices: 47.8 us -> none  [body(): lax.all_to_all(answers, ('sp', 'tp'), split_axis=0, concat_axis=0, tiled=...]
    dot_general x5 -> x0, matrix products: 17.4 us -> none  [the longest x1 10.1 us: expert_block(): jnp.einsum('...ecf,efd->...ecd', hidden, down_matrix, preferred_element_t...]
    all_to_all x1 -> x0, starting transfers between devices: 4.61 us -> none  [body(): lax.all_to_all(answers, ('sp', 'tp'), split_axis=0, concat_axis=0, tiled=...]
  transfers between devices with their start and end apart: 1 -> 0, of which waited for: 1 -> 0; matrix products, arithmetic and copies ran while one was open for 0% -> 0% of each run, Pallas kernels for 0% -> 0%
where the time goes in v1:
time: 133 us; the launch traced here: 131 us
  Pallas kernels  129 us (97%)
  local copies, waits for them, and re-layouts  1.88 us (1%)
    pallas_call x1, Pallas kernels, routed_experts(): pl.pallas_call(expert_kernel, in_specs=[vmem] * 4 + [anywhere] * 3, out_s...  102 us
    pallas_call x1, Pallas kernels, gated_arrivals(): pl.pallas_call(mixing_kernel, in_specs=[vmem] * 7 + [pl.BlockSpec(memory_...  27.8 us

profile of v1, /device:TPU:7, one launch (start us, length us, event | category | flops | bytes accessed | tf_op | source)
XLA Modules:
  0.0 131.4 jit_solution(11519662301200850622)
XLA Ops:
  0.0 27.8 %shard_map.145.stream_ref = bf16[128,2048]{1,0:T(8,128)(2,1)} custom-call(bf16[512,512]{1,0:T(8,128)(2,1)} %q_ref.1, bf16[512,512]{1,0:T(8,128)(2,1)} %f_ref.1, f32[1,512]{1,0:T(1,128)} %bitcast.8, f32[4,512]{1,0:T(4,128)} %bitcast.6, bf16[512,512]{1,0:T(8,128)(2,1)} %v_ref.1, bf16[512,512]{1,0:T(8,128)(2,1)} %g_ref.1, f32[1,512]{1,0:T(1,128)} %bitcast.9, ...), custom_call_target="tpu_custom_call" | custom-call | tf_op jit(solution)/shard_map/pallas_call | solution.py:199
  27.8 101.7 %shard_map.146 = bf16[128,2048]{1,0:T(8,128)(2,1)} custom-call(bf16[128,2048]{1,0:T(8,128)(2,1)} %shard_map.145.stream_ref, f32[1,2048]{1,0:T(1,128)} %bitcast.7, s32[2,128]{1,0:T(2,128)} %bitcast.10, f32[2,128]{1,0:T(2,128)} %bitcast.11, bf16[1,2048,1024]{2,1,0:T(8,128)(2,1)} %gate_ref.1, bf16[1,2048,1024]{2,1,0:T(8,128)(2,1)} %up_ref.1, ...), custom_call_target="tpu_custom_call" | custom-call | tf_op jit(solution)/shard_map/pallas_call | solution.py:478
  129.5 1.9 %copy.17 = bf16[128,2048]{1,0:T(8,128)(2,1)} copy(bf16[128,2048]{1,0:T(8,128)(2,1)} %shard_map.146) | data formatting | bytes 1048576

commit v2 on v1

--- a/solution.py
+++ b/solution.py
@@ -265,8 +265,13 @@
         copy.start()
         loads.append(copy)
 
+    bits = [1 << k for k in range(peers.bit_length() - 1)]
+    assert 1 << len(bits) == peers
+    flips = [(1 - 2 * lax.rem(spot // bit, 2)) * bit for bit in bits]
+
     def place(d):
-        other = lax.rem(spot + d, peers)
+        mask = d
+        other = spot + sum(lax.rem(mask // bit, 2) * flip for bit, flip in zip(bits, flips))
         return other, {"sp": side * near + other // mates, "tp": lax.rem(other, mates)}
 
     barrier = pltpu.get_barrier_semaphore()
@@ -410,18 +415,17 @@
 
     pack(0, whole)
     spread(pack_ref, came_ref, 0, whole, 0, out_send, out_recv)
+
+    note.wait_recv()
+    for c in range(CHUNKS):
+        over[c].wait_recv()
+        pack(1, parts[c])
+        spread(pack_ref, came_ref, 1, parts[c], 1 + c, out_send, out_recv)
     for copy in loads:
         copy.wait()
     arrive(pack_ref, came_ref, 0, whole, 0, out_send, out_recv)
     enter(0)
     leave(0, whole)
-    spread(answer_ref, back_ref, 0, whole, 0, ret_send, ret_recv)
-
-    note.wait_recv()
-    for c in range(CHUNKS):
-        over[c].wait_recv()
-        pack(1, parts[c])
-        spread(pack_ref, came_ref, 1, parts[c], 1 + c, out_send, out_recv)
     for c in range(CHUNKS):
         arrive(pack_ref, came_ref, 1, parts[c], 1 + c, out_send, out_recv)
     enter(1)
@@ -429,6 +433,7 @@
         leave(1, parts[c])
         spread(answer_ref, back_ref, 1, parts[c], 1 + c, ret_send, ret_recv)
 
+    spread(answer_ref, back_ref, 0, whole, 0, ret_send, ret_recv)
     home = []
     high, low = weights(1)
     for c in range(CHUNKS):

time: 133 us -> 116 us (0.87)
  Pallas kernels: 129 us -> 113 us
    pallas_call x1, Pallas kernels: 102 us -> 85.1 us  [routed_experts(): pl.pallas_call(expert_kernel, in_specs=[vmem] * 4 + [anywhere] * 3, out_s...]
where the time goes in v2:
time: 116 us; the launch traced here: 115 us
  Pallas kernels  113 us (97%)
  local copies, waits for them, and re-layouts  1.88 us (2%)
    pallas_call x1, Pallas kernels, routed_experts(): pl.pallas_call(expert_kernel, in_specs=[vmem] * 4 + [anywhere] * 3, out_s...  85.1 us
    pallas_call x1, Pallas kernels, gated_arrivals(): pl.pallas_call(mixing_kernel, in_specs=[vmem] * 7 + [pl.BlockSpec(memory_...  27.8 us

profile of v2, /device:TPU:7, one launch (start us, length us, event | category | flops | bytes accessed | tf_op | source)
XLA Modules:
  0.0 114.8 jit_solution(674693556708829310)
XLA Ops:
  0.0 27.8 %shard_map.145.stream_ref = bf16[128,2048]{1,0:T(8,128)(2,1)} custom-call(bf16[512,512]{1,0:T(8,128)(2,1)} %q_ref.1, bf16[512,512]{1,0:T(8,128)(2,1)} %f_ref.1, f32[1,512]{1,0:T(1,128)} %bitcast.8, f32[4,512]{1,0:T(4,128)} %bitcast.6, bf16[512,512]{1,0:T(8,128)(2,1)} %v_ref.1, bf16[512,512]{1,0:T(8,128)(2,1)} %g_ref.1, f32[1,512]{1,0:T(1,128)} %bitcast.9, ...), custom_call_target="tpu_custom_call" | custom-call | tf_op jit(solution)/shard_map/pallas_call | solution.py:199
  27.8 85.1 %shard_map.146 = bf16[128,2048]{1,0:T(8,128)(2,1)} custom-call(bf16[128,2048]{1,0:T(8,128)(2,1)} %shard_map.145.stream_ref, f32[1,2048]{1,0:T(1,128)} %bitcast.7, s32[2,128]{1,0:T(2,128)} %bitcast.10, f32[2,128]{1,0:T(2,128)} %bitcast.11, bf16[1,2048,1024]{2,1,0:T(8,128)(2,1)} %gate_ref.1, bf16[1,2048,1024]{2,1,0:T(8,128)(2,1)} %up_ref.1, ...), custom_call_target="tpu_custom_call" | custom-call | tf_op jit(solution)/shard_map/pallas_call | solution.py:483
  113.0 1.9 %copy.17 = bf16[128,2048]{1,0:T(8,128)(2,1)} copy(bf16[128,2048]{1,0:T(8,128)(2,1)} %shard_map.146) | data formatting | bytes 1048576
